TPU v7x, 32 devices: a whole 2x2x4 slice. The times are simulated.
32 devices in a mesh: ep: 4 (over y, x), tp: 8 (over z, core).
Axes of the slice: x: 2, y: 2, z: 4, core: 2. Of those that a mesh axis runs over, the one named last changes fastest.
Arguments:
- pool_in: bfloat16 [16384, 1024], P(('ep', 'tp')), may hold values from -6 to 6
- pool_weight: bfloat16 [4, 256, 256], replicated, may hold values from -0.375 to 0.375
- pool_gain: float32 [1024], replicated, may hold values from 0.1 to 1.9
- out_weight: bfloat16 [1024, 2048], P('tp'), may hold values from -0.1875 to 0.1875
- mix_gain: float32 [2048], replicated, may hold values from 0.1 to 1.9
- expert_in: bfloat16 [1024, 2048], P('ep'), may hold values from -6 to 6
- routes: int32 [1024, 4], P('ep'), may hold values from 0 to 7, all different within a row; in each aligned block of 32 rows (0 to 31, 32 to 63, ...) at most 32 rows name the same one
- route_weight: float32 [1024, 4], P('ep'), may hold values from 0.1 to 1
- pre_gain: float32 [2048], replicated, may hold values from 0.1 to 1.9
- gate_weight: bfloat16 [8, 2048, 4096], P('ep', None, 'tp'), may hold values from -0.39648438 to 0.39648438
- up_weight: bfloat16 [8, 2048, 4096], P('ep', None, 'tp'), may hold values from -0.39648438 to 0.39648438
- down_weight: bfloat16 [8, 4096, 2048], P('ep', 'tp'), may hold values from -0.09375 to 0.09375
- post_gain: float32 [2048], replicated, may hold values from 0.1 to 1.9
Outputs:
- mix_out: bfloat16 [16384, 2048], P(('ep', 'tp'))
- expert_out: bfloat16 [1024, 2048], P(('ep', 'tp'))
Inputs may be any that keep to these rules, and one draw needn't show every extreme that they name: `routes`: each row names 4 different experts. In each aligned block of 32 rows no expert is named by more than 32 rows, a bound that some block reaches.
All inputs are finite; a program needn't handle non-finite values.
Results may differ from a plain program's by a relative error of at most 0.019.
Values may be sent and summed in bfloat16 or wider, within the bound.
A program may use at most 128 MiB of HBM per device.

v0:
```python
import jax
import jax.numpy as jnp
from jax import lax
from jax.sharding import PartitionSpec as P

WINDOWS = (2, 4, 8, 16)
EPS = 1e-06
LIMIT = 7.0
ALPHA = 1.702


def shifted(block, axis, distance):
    devices = range(lax.axis_size(axis))
    route = [(i - distance, i) for i in devices if i - distance in devices]
    return lax.ppermute(block, axis, route)


def rms_scale(values, gain):
    mean_square = jnp.mean(values * values, axis=-1, keepdims=True)
    return values * lax.rsqrt(mean_square + EPS) * gain


def trailing_pool(padded, first_pos, rows):
    group = padded.shape[1] // 4
    position = first_pos + jnp.arange(rows, dtype=jnp.int32)
    pieces = []
    for which, window in enumerate(WINDOWS):
        channels = padded[:, which * group : (which + 1) * group]
        running = channels[16 : 16 + rows]
        for reach in range(2, window + 1):
            running = running + channels[17 - reach : 17 - reach + rows]
        count = jnp.minimum(position + 1, window).astype(jnp.float32)[:, None]
        pieces.append(running / count)
    pooled = jnp.concatenate(pieces, axis=1)
    return (pooled - padded[16:]).astype(jnp.bfloat16)


def expert_weights(routes, route_weight, experts):
    chosen = routes[:, :, None] == jnp.arange(experts, dtype=jnp.int32)[None, None, :]
    return jnp.sum(jnp.where(chosen, route_weight[:, :, None], 0.0), axis=1)


def clamped_unit(gate, up):
    gate = jnp.minimum(gate, LIMIT)
    up = jnp.clip(up, -LIMIT, LIMIT)
    return (up + 1.0) * gate * jax.nn.sigmoid(ALPHA * gate)


def body(
    pool_in,
    pool_weight,
    pool_gain,
    out_weight,
    mix_gain,
    expert_in,
    routes,
    route_weight,
    pre_gain,
    gate_weight,
    up_weight,
    down_weight,
    post_gain,
):
    rows, channels = pool_in.shape
    width = out_weight.shape[1]
    rim = shifted(pool_in[rows - 16 :], ("ep", "tp"), 1)
    padded = jnp.concatenate([rim, pool_in], axis=0).astype(jnp.float32)
    first_pos = (lax.axis_index("ep") * lax.axis_size("tp") + lax.axis_index("tp")) * rows
    diff = trailing_pool(padded, first_pos, rows)
    mixed = jnp.einsum(
        "sgc,gcd->sgd",
        diff.reshape(rows, 4, channels // 4),
        pool_weight,
        preferred_element_type=jnp.float32,
    )
    mixed = (mixed.reshape(rows, channels) * pool_gain).astype(jnp.bfloat16)
    projected = jnp.dot(
        mixed,
        lax.all_gather(out_weight, "tp", axis=0, tiled=True),
        preferred_element_type=jnp.float32,
    )
    mix_out = rms_scale(projected, mix_gain).astype(jnp.bfloat16)
    ep_place = lax.axis_index("ep")
    local_experts = gate_weight.shape[0]
    experts = local_experts * lax.axis_size("ep")
    weights = expert_weights(routes, route_weight, experts)
    weights = lax.all_gather(weights, "ep", axis=0, tiled=True)
    weights = lax.dynamic_slice_in_dim(weights, ep_place * local_experts, local_experts, 1)
    normed = rms_scale(expert_in.astype(jnp.float32), pre_gain).astype(jnp.bfloat16)
    normed = lax.all_gather(normed, "ep", axis=0, tiled=True)
    hidden = []
    for which in range(local_experts):
        gate = jnp.dot(normed, gate_weight[which], preferred_element_type=jnp.float32)
        up = jnp.dot(normed, up_weight[which], preferred_element_type=jnp.float32)
        hidden.append((clamped_unit(gate, up) * weights[:, which : which + 1]).astype(jnp.bfloat16))
    hidden = jnp.concatenate(hidden, axis=1)
    partial = jnp.dot(
        hidden, down_weight.reshape(-1, width), preferred_element_type=jnp.float32
    ).astype(jnp.bfloat16)
    combined = lax.psum_scatter(partial, ("ep", "tp"), scatter_dimension=0, tiled=True).astype(
        jnp.float32
    )
    expert_out = rms_scale(combined, post_gain).astype(jnp.bfloat16)
    return (mix_out, expert_out)


def solution(mesh):
    return jax.shard_map(
        body,
        mesh=mesh,
        in_specs=(
            P(("ep", "tp"), None),
            P(),
            P(),
            P("tp", None),
            P(),
            P("ep", None),
            P("ep", None),
            P("ep", None),
            P(),
            P("ep", None, "tp"),
            P("ep", None, "tp"),
            P("ep", "tp", None),
            P(),
        ),
        out_specs=(P(("ep", "tp"), None), P(("ep", "tp"), None)),
        check_vma=False,
    )
```

profile of v0, /device:TPU:0, one launch (start us, length us, event | category | flops | bytes accessed | tf_op | source)
XLA Modules:
  0.0 269.7 jit_solution(13656059231238334772)
XLA Ops:
  7.2 1.6 fusion
  8.8 2.5 fusion.2
  11.4 0.7 all-gather.3.cloned.1.call-update
  12.2 9.7 %all_gather.11 = f32[1024,8]{0,1:T(8,128)S(1)} all-gather(f32[256,8]{0,1:T(8,128)S(1)} %select_reduce_fusion), channel_id=1, replica_groups=mesh['ep'=4,'tp'=8] {'ep'}, dimensions={0}, use_global_device_ids=true | all-gather | bytes 40960 | tf_op jit(solution)/shard_map/all_gather | solution.py:87
  21.9 44.9 %all-gather.5.cloned.1.call-done = bf16[1024,2048]{1,0:T(8,128)(2,1)} async-done(((bf16[256,2048]{1,0:T(8,128)(2,1)}), bf16[1024,2048]{1,0:T(8,128)(2,1)}) %all-gather.5.cloned.1.call-update) | async-done | bytes 4194320 | tf_op jit(solution)/shard_map/all_gather | solution.py:90
  66.8 5.4 %fusion.10 = f32[1024,512]{0,1:T(8,128)S(1)} fusion(bf16[1024,2048]{1,0:T(8,128)(2,1)} %all-gather.5.cloned.1.call-done, bf16[2,2048,512]{2,1,0:T(8,128)(2,1)} %param.23), kind=kOutput, calls=%fused_computation.17 | convolution fusion | flops 2147483648 | bytes 8388608 | tf_op jit(solution)/shard_map/dot_general | solution.py:94
  72.2 2.4 fusion.14
  74.6 3.0 %multiply_convert_fusion.1 = bf16[1024,512]{0,1:T(8,128)(2,1)S(1)} fusion(f32[1024,512]{0,1:T(8,128)S(1)} %fusion.10, bf16[1024,2048]{1,0:T(8,128)(2,1)S(1)} %copy-done.10, bf16[2,2048,512]{2,1,0:T(8,128)(2,1)S(1)} %copy-done.8, f32[1024]{0:T(1024)S(1)} %bitcast.39), kind=kOutput, calls=%fused_computation.23 | convolution fusion | flops 2153250816 | bytes 9441280 | tf_op jit(solution)/shard_map/dot_general | solution.py:93
  77.7 3.0 %multiply_convert_fusion.2 = bf16[1024,512]{0,1:T(8,128)(2,1)S(1)} fusion(f32[1024,512]{0,1:T(8,128)S(1)} %fusion.14, bf16[1024,2048]{1,0:T(8,128)(2,1)S(1)} %copy-done.10, bf16[2,2048,512]{2,1,0:T(8,128)(2,1)S(1)} %copy-done.8, f32[1024]{0:T(1024)S(1)} %bitcast.38), kind=kOutput, calls=%fused_computation.26 | convolution fusion | flops 2153250816 | bytes 9441280 | tf_op jit(solution)/shard_map/dot_general | solution.py:93
  80.7 6.5 %convolution_convert_fusion = bf16[1024,2048]{1,0:T(8,128)(2,1)} fusion(bf16[1024,2048]{1,0:T(8,128)(2,1)S(1)} %bitcast.40, bf16[1024,512]{0,1:T(8,128)(2,1)S(1)} %multiply_convert_fusion.1, bf16[1024,512]{0,1:T(8,128)(2,1)S(1)} %multiply_convert_fusion.2), kind=kOutput, calls=%fused_computation.2 | convolution fusion | flops 4301258752 | bytes 10485760 | tf_op jit(solution)/shard_map/dot_general | solution.py:97
  87.2 1.2 copy-done.1
  88.4 1.5 collective-permute-start
  90.0 0.8 collective-permute-done
  90.8 0.2 maximum_convert_fusion
  91.0 0.6 fusion.27
  91.7 0.6 fusion.30
  92.3 0.4 fusion.3
  92.8 0.5 fusion.24
  93.7 22.0 %all-gather.3.cloned.1.call-done = bf16[1024,2048]{1,0:T(8,128)(2,1)} async-done(((bf16[128,2048]{1,0:T(8,128)(2,1)}), bf16[1024,2048]{1,0:T(8,128)(2,1)}) %all-gather.3.cloned.1.call-update) | async-done | bytes 4194320 | tf_op jit(solution)/shard_map/all_gather | solution.py:79
  115.6 4.7 %multiply_reduce_fusion = (f32[512]{0:T(512)S(1)}, f32[512,2048]{1,0:T(8,128)S(1)}) fusion(bf16[512,1024]{0,1:T(8,128)(2,1)S(1)} %fusion.7, bf16[1024,2048]{1,0:T(8,128)(2,1)} %all-gather.3.cloned.1.call-done), kind=kOutput, calls=%fused_computation.1 | convolution fusion | flops 2149580288 | bytes 9439232 | tf_op jit(solution)/shard_map/dot_general | solution.py:77
  120.3 1.7 multiply_convert_fusion
  122.1 138.4 %reduce-scatter.2.cloned.1.call-done = bf16[32,2048]{1,0:T(8,128)(2,1)} async-done(((bf16[1024,2048]{1,0:T(8,128)(2,1)}), bf16[32,2048]{1,0:T(8,128)(2,1)}) %reduce-scatter.2.cloned.1.call-update) | async-done | bytes 131088 | tf_op jit(solution)/shard_map/reduce_scatter | solution.py:100
  260.5 1.0 fusion.31
  261.6 1.7 fusion.33
  (35 shorter events, 0.6 us)
Async XLA Ops:
  7.2 85.6 %copy-start = (bf16[4,256,256]{2,1,0:T(8,128)(2,1)S(1)}, bf16[4,256,256]{2,1,0:T(8,128)(2,1)}, u32[]{:S(2)}) copy-start(bf16[4,256,256]{2,1,0:T(8,128)(2,1)} %param.14) | copy-start | bytes 1572868
  7.2 59.6 %all-gather.5.cloned.1.call-start = ((), (), s32[]{:S(2)}) async-start(), calls=%async_computation.2 | async-start | bytes 5242880 | tf_op jit(solution)/shard_map/all_gather | solution.py:90
  8.8 3.4 %copy-start.5 = (f32[256,4]{0,1:T(4,128)S(1)}, f32[256,4]{0,1:T(4,128)}, u32[]{:S(2)}) copy-start(f32[256,4]{0,1:T(4,128)} %param.20) | copy-start | bytes 12292
  8.8 3.4 %copy-start.6 = (s32[256,4]{0,1:T(4,128)S(1)}, s32[256,4]{0,1:T(4,128)}, u32[]{:S(2)}) copy-start(s32[256,4]{0,1:T(4,128)} %param.19) | copy-start | bytes 12292
  11.3 104.3 %all-gather.3.cloned.1.call-start = ((), (), s32[]{:S(2)}) async-start(), calls=%async_computation.1 | async-start | bytes 4718592 | tf_op jit(solution)/shard_map/all_gather | solution.py:79
  12.1 248.4 %reduce-scatter.2.cloned.1.call-start = ((), (), s32[]{:S(2)}) async-start(), calls=%async_computation.3 | async-start | bytes 4325376 | tf_op jit(solution)/shard_map/reduce_scatter | solution.py:100
  66.8 5.4 %copy-start.7 = (bf16[2,2048,512]{2,1,0:T(8,128)(2,1)S(1)}, bf16[2,2048,512]{2,1,0:T(8,128)(2,1)}, u32[]{:S(2)}) copy-start(bf16[2,2048,512]{2,1,0:T(8,128)(2,1)} %param.23) | copy-start | bytes 12582916
  66.8 5.4 %copy-start.10 = (bf16[1024,2048]{1,0:T(8,128)(2,1)S(1)}, bf16[1024,2048]{1,0:T(8,128)(2,1)}, u32[]{:S(2)}) copy-start(bf16[1024,2048]{1,0:T(8,128)(2,1)} %all-gather.5.cloned.1.call-done) | copy-start | bytes 12582916
  72.2 2.4 copy-start.8
  77.6 3.0 %copy-start.9 = (bf16[2,512,2048]{2,1,0:T(8,128)(2,1)S(1)}, bf16[2,512,2048]{2,1,0:T(8,128)(2,1)}, u32[]{:S(2)}) copy-start(bf16[2,512,2048]{2,1,0:T(8,128)(2,1)} %param.24) | copy-start | bytes 12582916
  87.1 1.3 copy-start.1
  88.4 2.4 collective-permute-start
  92.7 0.7 copy-start.4
  93.6 26.7 %copy-start.2 = (f32[2048]{0:T(1024)S(1)}, f32[2048]{0:T(1024)}, u32[]{:S(2)}) copy-start(f32[2048]{0:T(1024)} %param.17) | copy-start | bytes 24580
  120.3 141.2 %copy-start.3 = (f32[2048]{0:T(1024)S(1)}, f32[2048]{0:T(1024)}, u32[]{:S(2)}) copy-start(f32[2048]{0:T(1024)} %param.25) | copy-start | bytes 24580
Sparse Core Ops, SparseCore 0:
  11.5 55.2 all-gather.4
  68.4 47.2 all-gather.2
  117.9 142.5 reduce-scatter.1
where the time goes:
time: 270 us
  waiting for transfers between devices  207 us (77%)
  matrix products  25.4 us (9%)
  between operations  14 us (5%)
  other arithmetic  10.7 us (4%)
  blocking collectives  9.67 us (4%)
    reduce_scatter x1, waiting for transfers between devices, body(): lax.psum_scatter(partial, ('ep', 'tp'), scatter_dimension=0, tiled=True)  138 us
    all_gather x1, waiting for transfers between devices, body(): normed = lax.all_gather(normed, 'ep', axis=0, tiled=True)  44.9 us
    all_gather x1, waiting for transfers between devices, body(): lax.all_gather(out_weight, 'tp', axis=0, tiled=True)  22 us
    all_gather x1, blocking collectives, body(): weights = lax.all_gather(weights, 'ep', axis=0, tiled=True)  9.67 us
    dot_general x2, matrix products, body(): up = jnp.dot(normed, up_weight[which], preferred_element_type=jnp.float32)  7.79 us
    dot_general x1, matrix products, body(): jnp.dot(hidden, down_weight.reshape(-1, width), preferred_element_type=jn...  6.47 us
    dot_general x2, matrix products, body(): jnp.dot(normed, gate_weight[which], preferred_element_type=jnp.float32)  5.99 us
  transfers between devices with their start and end apart: 4, of which 4 were waited for; matrix products, arithmetic and copies ran while one was open for 11% of the time, Pallas kernels for 0%

commit v1 on v0

--- a/solution.py
+++ b/solution.py
@@ -7,6 +7,13 @@
 EPS = 1e-06
 LIMIT = 7.0
 ALPHA = 1.702
+
+
+def unite_the_entries(mine_x, row_axis, in_dim):
+    r1 = lax.axis_size(row_axis)
+    far_arr = jnp.stack([mine_x] * r1, axis=0)
+    part_next = lax.all_to_all(far_arr, row_axis, 0, 0)
+    return jnp.concatenate(part_next, axis=in_dim)
 
 
 def shifted(block, axis, distance):
@@ -75,9 +82,7 @@
     )
     mixed = (mixed.reshape(rows, channels) * pool_gain).astype(jnp.bfloat16)
     projected = jnp.dot(
-        mixed,
-        lax.all_gather(out_weight, "tp", axis=0, tiled=True),
-        preferred_element_type=jnp.float32,
+        mixed, unite_the_entries(out_weight, "tp", 0), preferred_element_type=jnp.float32
     )
     mix_out = rms_scale(projected, mix_gain).astype(jnp.bfloat16)
     ep_place = lax.axis_index("ep")

time: 270 us -> 242 us (0.90)
  waiting for transfers between devices: 207 us -> 171 us
  starting transfers between devices: 1.64 us -> 8.12 us
    reduce_scatter x1, waiting for transfers between devices: 138 us -> 99.1 us  [body(): lax.psum_scatter(partial, ('ep', 'tp'), scatter_dimension=0, tiled=True)]
    all_to_all x0 -> x1, waiting for transfers between devices: none -> 33.3 us  [unite_the_entries(): part_next = lax.all_to_all(far_arr, row_axis, 0, 0)]
    all_gather x1 -> x0, waiting for transfers between devices: 22 us -> none  [body(): lax.all_gather(out_weight, 'tp', axis=0, tiled=True)]
    all_gather x1, waiting for transfers between devices: 44.9 us -> 37.9 us  [body(): normed = lax.all_gather(normed, 'ep', axis=0, tiled=True)]
    all_to_all x0 -> x1, starting transfers between devices: none -> 6.49 us  [unite_the_entries(): part_next = lax.all_to_all(far_arr, row_axis, 0, 0)]
  transfers between devices with their start and end apart: 4 -> 4, of which waited for: 4 -> 4; matrix products, arithmetic and copies ran while one was open for 11% -> 13% of each run, Pallas kernels for 0% -> 0%
where the time goes in v1:
time: 242 us
  waiting for transfers between devices  171 us (71%)
  matrix products  25.4 us (10%)
  between operations  14.3 us (6%)
  other arithmetic  10.5 us (4%)
  blocking collectives  8.7 us (4%)
  starting transfers between devices  8.12 us (3%)
  local copies, waits for them, and re-layouts  3.79 us (2%)
    reduce_scatter x1, waiting for transfers between devices, body(): lax.psum_scatter(partial, ('ep', 'tp'), scatter_dimension=0, tiled=True)  99.1 us
    all_gather x1, waiting for transfers between devices, body(): normed = lax.all_gather(normed, 'ep', axis=0, tiled=True)  37.9 us
    all_to_all x1, waiting for transfers between devices, unite_the_entries(): part_next = lax.all_to_all(far_arr, row_axis, 0, 0)  33.3 us
    all_gather x1, blocking collectives, body(): weights = lax.all_gather(weights, 'ep', axis=0, tiled=True)  8.7 us
    dot_general x2, matrix products, body(): up = jnp.dot(normed, up_weight[which], preferred_element_type=jnp.float32)  7.78 us
    all_to_all x1, starting transfers between devices, unite_the_entries(): part_next = lax.all_to_all(far_arr, row_axis, 0, 0)  6.49 us
    dot_general x1, matrix products, body(): jnp.dot(hidden, down_weight.reshape(-1, width), preferred_element_type=jn...  6.45 us
    dot_general x2, matrix products, body(): jnp.dot(normed, gate_weight[which], preferred_element_type=jnp.float32)  5.99 us
  transfers between devices with their start and end apart: 4, of which 4 were waited for; matrix products, arithmetic and copies ran while one was open for 13% of the time, Pallas kernels for 0%

profile of v1, /device:TPU:0, one launch (start us, length us, event | category | flops | bytes accessed | tf_op | source)
XLA Modules:
  0.0 241.8 jit_solution(7534253019966431960)
XLA Ops:
  7.2 1.6 fusion
  8.8 2.5 %fusion.2 = bf16[256,2048]{1,0:T(8,128)(2,1)} fusion(bf16[256,2048]{1,0:T(8,128)(2,1)} %param.18, f32[2048]{0:T(1024)} %param.21, f32[256]{0:T(256)S(1)} %add_rsqrt_fusion.1), kind=kLoop, calls=%fused_computation.7 | loop fusion | flops 2097152 | bytes 2106368 | tf_op jit(solution)/shard_map/convert_element_type | solution.py:94
  11.4 2.5 %stack.2 = bf16[8,128,2048]{2,1,0:T(8,128)(2,1)} broadcast(bf16[128,2048]{1,0:T(8,128)(2,1)S(1)} %copy-done.2), dimensions={1,2} | broadcast | bytes 4718592 | tf_op jit(solution)/shard_map/stack | solution.py:14
  13.9 6.5 %all-to-all-start = ((bf16[8,128,2048]{2,1,0:T(8,128)(2,1)}), bf16[8,128,2048]{2,1,0:T(8,128)(2,1)}, u32[]{:S(2)}, u32[]{:S(2)}) async-start(bf16[8,128,2048]{2,1,0:T(8,128)(2,1)} %stack.2), calls=%async_computation | async-start | bytes 8388608 | tf_op jit(solution)/shard_map/all_to_all | solution.py:15
  20.5 8.7 %all_gather.7 = f32[1024,8]{0,1:T(8,128)S(1)} all-gather(f32[256,8]{0,1:T(8,128)S(1)} %select_reduce_fusion), channel_id=1, replica_groups=mesh['ep'=4,'tp'=8] {'ep'}, dimensions={0}, use_global_device_ids=true | all-gather | bytes 40960 | tf_op jit(solution)/shard_map/all_gather | solution.py:92
  29.2 37.9 %all-gather.2.cloned.1.call-done = bf16[1024,2048]{1,0:T(8,128)(2,1)} async-done(((bf16[256,2048]{1,0:T(8,128)(2,1)}), bf16[1024,2048]{1,0:T(8,128)(2,1)}) %all-gather.2.cloned.1.call-update) | async-done | bytes 4194320 | tf_op jit(solution)/shard_map/all_gather | solution.py:95
  67.1 5.4 %fusion.9 = f32[1024,512]{0,1:T(8,128)S(1)} fusion(bf16[1024,2048]{1,0:T(8,128)(2,1)} %all-gather.2.cloned.1.call-done, bf16[2,2048,512]{2,1,0:T(8,128)(2,1)} %param.23), kind=kOutput, calls=%fused_computation.15 | convolution fusion | flops 2147483648 | bytes 8388608 | tf_op jit(solution)/shard_map/dot_general | solution.py:99
  72.5 2.4 fusion.13
  74.9 3.0 %multiply_convert_fusion.1 = bf16[1024,512]{0,1:T(8,128)(2,1)S(1)} fusion(f32[1024,512]{0,1:T(8,128)S(1)} %fusion.9, bf16[1024,2048]{1,0:T(8,128)(2,1)S(1)} %copy-done.11, bf16[2,2048,512]{2,1,0:T(8,128)(2,1)S(1)} %copy-done.9, f32[1024]{0:T(1024)S(1)} %bitcast.38), kind=kOutput, calls=%fused_computation.21 | convolution fusion | flops 2153250816 | bytes 9441280 | tf_op jit(solution)/shard_map/dot_general | solution.py:98
  77.9 3.0 %multiply_convert_fusion.2 = bf16[1024,512]{0,1:T(8,128)(2,1)S(1)} fusion(f32[1024,512]{0,1:T(8,128)S(1)} %fusion.13, bf16[1024,2048]{1,0:T(8,128)(2,1)S(1)} %copy-done.11, bf16[2,2048,512]{2,1,0:T(8,128)(2,1)S(1)} %copy-done.9, f32[1024]{0:T(1024)S(1)} %bitcast.37), kind=kOutput, calls=%fused_computation.24 | convolution fusion | flops 2153250816 | bytes 9441280 | tf_op jit(solution)/shard_map/dot_general | solution.py:98
  81.0 6.5 %convolution_convert_fusion = bf16[1024,2048]{1,0:T(8,128)(2,1)} fusion(bf16[1024,2048]{1,0:T(8,128)(2,1)S(1)} %bitcast.39, bf16[1024,512]{0,1:T(8,128)(2,1)S(1)} %multiply_convert_fusion.1, bf16[1024,512]{0,1:T(8,128)(2,1)S(1)} %multiply_convert_fusion.2), kind=kOutput, calls=%fused_computation.2 | convolution fusion | flops 4301258752 | bytes 10485760 | tf_op jit(solution)/shard_map/dot_general | solution.py:102
  87.4 1.2 copy-done.1
  88.6 1.6 collective-permute-start
  90.3 0.8 collective-permute-done
  91.3 0.6 fusion.25
  91.9 0.6 fusion.28
  92.6 0.4 fusion.3
  93.0 0.5 multiply_convert_fusion.3
  93.5 33.3 %all-to-all-done = bf16[8,128,2048]{2,1,0:T(8,128)(2,1)} async-done(((bf16[8,128,2048]{2,1,0:T(8,128)(2,1)}), bf16[8,128,2048]{2,1,0:T(8,128)(2,1)}, u32[]{:S(2)}, u32[]{:S(2)}) %all-to-all-start) | async-done | bytes 4194336 | tf_op jit(solution)/shard_map/all_to_all | solution.py:15
  126.8 4.7 %multiply_reduce_fusion = (f32[512]{0:T(512)S(1)}, f32[512,2048]{1,0:T(8,128)S(1)}) fusion(bf16[512,1024]{0,1:T(8,128)(2,1)S(1)} %bitcast.35, bf16[1024,2048]{1,0:T(8,128)(2,1)} %bitcast.2), kind=kOutput, calls=%fused_computation.1 | convolution fusion | flops 2149580288 | bytes 9439232 | tf_op jit(solution)/shard_map/dot_general | solution.py:84
  131.5 1.7 multiply_convert_fusion
  133.2 99.1 %reduce-scatter.2.cloned.1.call-done = bf16[32,2048]{1,0:T(8,128)(2,1)} async-done(((bf16[1024,2048]{1,0:T(8,128)(2,1)}), bf16[32,2048]{1,0:T(8,128)(2,1)}) %reduce-scatter.2.cloned.1.call-update) | async-done | bytes 131088 | tf_op jit(solution)/shard_map/reduce_scatter | solution.py:105
  232.3 1.0 fusion.29
  233.3 1.7 fusion.31
  (37 shorter events, 0.5 us)
Async XLA Ops:
  7.2 85.8 %copy-start = (bf16[4,256,256]{2,1,0:T(8,128)(2,1)S(1)}, bf16[4,256,256]{2,1,0:T(8,128)(2,1)}, u32[]{:S(2)}) copy-start(bf16[4,256,256]{2,1,0:T(8,128)(2,1)} %param.14) | copy-start | bytes 1572868
  7.2 4.2 %copy-start.2 = (bf16[128,2048]{1,0:T(8,128)(2,1)S(1)}, bf16[128,2048]{1,0:T(8,128)(2,1)}, u32[]{:S(2)}) copy-start(bf16[128,2048]{1,0:T(8,128)(2,1)} %param.16) | copy-start | bytes 1572868
  7.2 59.9 %all-gather.2.cloned.1.call-start = ((), (), s32[]{:S(2)}) async-start(), calls=%async_computation.2 | async-start | bytes 5242880 | tf_op jit(solution)/shard_map/all_gather | solution.py:95
  13.9 6.5 %copy-start.6 = (f32[256,4]{0,1:T(4,128)S(1)}, f32[256,4]{0,1:T(4,128)}, u32[]{:S(2)}) copy-start(f32[256,4]{0,1:T(4,128)} %param.20) | copy-start | bytes 12292
  13.9 6.6 %copy-start.7 = (s32[256,4]{0,1:T(4,128)S(1)}, s32[256,4]{0,1:T(4,128)}, u32[]{:S(2)}) copy-start(s32[256,4]{0,1:T(4,128)} %param.19) | copy-start | bytes 12292
  13.9 112.9 %all-to-all-start = ((bf16[8,128,2048]{2,1,0:T(8,128)(2,1)}), bf16[8,128,2048]{2,1,0:T(8,128)(2,1)}, u32[]{:S(2)}, u32[]{:S(2)}) async-start(bf16[8,128,2048]{2,1,0:T(8,128)(2,1)} %stack.2), calls=%async_computation | async-start | bytes 8388608 | tf_op jit(solution)/shard_map/all_to_all | solution.py:15
  20.4 211.9 %reduce-scatter.2.cloned.1.call-start = ((), (), s32[]{:S(2)}) async-start(), calls=%async_computation.3 | async-start | bytes 4325376 | tf_op jit(solution)/shard_map/reduce_scatter | solution.py:105
  67.1 5.4 %copy-start.8 = (bf16[2,2048,512]{2,1,0:T(8,128)(2,1)S(1)}, bf16[2,2048,512]{2,1,0:T(8,128)(2,1)}, u32[]{:S(2)}) copy-start(bf16[2,2048,512]{2,1,0:T(8,128)(2,1)} %param.23) | copy-start | bytes 12582916
  67.1 5.4 %copy-start.11 = (bf16[1024,2048]{1,0:T(8,128)(2,1)S(1)}, bf16[1024,2048]{1,0:T(8,128)(2,1)}, u32[]{:S(2)}) copy-start(bf16[1024,2048]{1,0:T(8,128)(2,1)} %all-gather.2.cloned.1.call-done) | copy-start | bytes 12582916
  72.5 2.4 %copy-start.9 = (bf16[2,2048,512]{2,1,0:T(8,128)(2,1)S(1)}, bf16[2,2048,512]{2,1,0:T(8,128)(2,1)}, u32[]{:S(2)}) copy-start(bf16[2,2048,512]{2,1,0:T(8,128)(2,1)} %param.22) | copy-start | bytes 12582916
  77.9 3.0 %copy-start.10 = (bf16[2,512,2048]{2,1,0:T(8,128)(2,1)S(1)}, bf16[2,512,2048]{2,1,0:T(8,128)(2,1)}, u32[]{:S(2)}) copy-start(bf16[2,512,2048]{2,1,0:T(8,128)(2,1)} %param.24) | copy-start | bytes 12582916
  87.4 1.2 copy-start.1
  87.4 2.8 %copy-start.5 = (f32[1024]{0:T(1024)S(1)}, f32[1024]{0:T(1024)}, u32[]{:S(2)}) copy-start(f32[1024]{0:T(1024)} %param.15) | copy-start | bytes 12292
  88.6 2.4 collective-permute-start
  126.8 4.7 %copy-start.3 = (f32[2048]{0:T(1024)S(1)}, f32[2048]{0:T(1024)}, u32[]{:S(2)}) copy-start(f32[2048]{0:T(1024)} %param.17) | copy-start | bytes 24580
  131.5 101.9 %copy-start.4 = (f32[2048]{0:T(1024)S(1)}, f32[2048]{0:T(1024)}, u32[]{:S(2)}) copy-start(f32[2048]{0:T(1024)} %param.25) | copy-start | bytes 24580
Sparse Core Ops, SparseCore 0:
  11.5 55.5 all-gather.1
  87.6 144.6 reduce-scatter.1
